TPU v7x, 512 devices: a whole 4x8x8 slice. The times are simulated.
512 devices in a mesh: sp: 32 (over z, x), tp: 16 (over y, core).
Axes of the slice: x: 4, y: 8, z: 8, core: 2. Of those that a mesh axis runs over, the one named last changes fastest.
Arguments:
- residual_layer_input: bfloat16 [8192, 2048], P(('sp', 'tp')), may hold values from -6 to 6
- value_projected: bfloat16 [8192, 4096], P('sp', 'tp'), may hold values from -6 to 6
- key_projected: bfloat16 [8192, 2048], P('sp', 'tp'), may hold values from -6 to 6
- query_projected: bfloat16 [8192, 2048], P('sp', 'tp'), may hold values from -6 to 6
- output_gate_projected: bfloat16 [8192, 4096], P('sp', 'tp'), may hold values from -6 to 6
- step_projected_raw: bfloat16 [2, 8192, 64], P(None, 'sp', 'tp'), may hold values from -5.5 to 5
- head_decay_logarithm: float32 [2, 64], P(None, 'tp'), may hold values from -15 to -2.9
- position_extra_decay: float32 [8192, 64], P('sp', 'tp'), may hold values from -2.1 to 0
- value_filter_weight: bfloat16 [5, 4096], P(None, 'tp'), may hold values from -2.5 to 2.5
- key_filter_weight: bfloat16 [5, 2048], P(None, 'tp'), may hold values from -2.5 to 2.5
- query_filter_weight: bfloat16 [5, 2048], P(None, 'tp'), may hold values from -2.5 to 2.5
- head_norm_gain: float32 [4096], P('tp'), may hold values from 0.1 to 1.9
- mixer_output_matrix: bfloat16 [4096, 2048], P(None, 'tp'), may hold values from -0.09375 to 0.09375
- expert_norm_gain: float32 [2048], replicated, may hold values from 0.1 to 1.9
- routes: int32 [8192, 2], P('sp'), may hold values from 0 to 31, all different within a row; in each aligned block of 16 rows (0 to 15, 16 to 31, ...) at most 2 rows name the same one
- chosen_expert_weight: float32 [8192, 2], P(('sp', 'tp')), may hold values from 0.1 to 1
- expert_gate_matrix: bfloat16 [32, 2048, 4096], P('sp', None, 'tp'), may hold values from -0.125 to 0.125
- expert_up_matrix: bfloat16 [32, 2048, 4096], P('sp', None, 'tp'), may hold values from -0.125 to 0.125
- expert_down_matrix: bfloat16 [32, 4096, 2048], P('sp', 'tp'), may hold values from -0.09375 to 0.09375
Outputs:
- layer_output: bfloat16 [8192, 2048], P(('sp', 'tp'))
Inputs may be any that keep to these rules, and one draw needn't show every extreme that they name: `routes`: each row names 2 different experts; the rows of one device (aligned blocks of 16 rows) name one expert 2 times at most, and that most is reached.
All inputs are finite; a program needn't handle non-finite values.
Results may differ from a plain program's by a relative error of at most 0.015.
Values may be sent and summed in bfloat16 or wider, within the bound.
A program may use at most 64 MiB of HBM per device.

v0:
```python
import jax
import jax.numpy as jnp
from jax import lax
from jax.sharding import Mesh
from jax.sharding import PartitionSpec as P

HEAD_DIM = 64
STATE = 128
BLOCK = 128
TAPS = 5
SP = ("sp_0", "sp_1")
TP = ("tp_0", "tp_1")
SP_TP = ("sp_0", "sp_1", "tp_0", "tp_1")
epsilon = 1e-06


def padded_2(cells, sides, width):
    for axis, dim in sides:
        count = lax.axis_size(axis)
        ends = count - 1
        head = lax.slice_in_dim(cells, 0, width, axis=dim)
        tail = lax.slice_in_dim(cells, cells.shape[dim] - width, cells.shape[dim], axis=dim)
        cells = jnp.concatenate(
            [
                lax.ppermute(tail, axis, [(i, (i + 1) % count) for i in range(ends)]),
                cells,
                lax.ppermute(head, axis, [((i + 1) % count, i) for i in range(ends)]),
            ],
            axis=dim,
        )
    return cells


def filled_with(x, identity):
    return jax.tree.map(
        lambda part, zero: jnp.zeros_like(part) + jnp.asarray(zero, part.dtype), x, identity
    )


def carried_in(x, axes, combine, identity, reverse):
    before = start = filled_with(x, identity)
    so_far = x
    for axis in reversed(axes):
        count, here = (lax.axis_size(axis), lax.axis_index(axis))
        pieces = jax.tree.map(
            lambda part, kind: lax.all_gather(part.astype(kind), axis),
            so_far,
            (jnp.bfloat16, jnp.bfloat16),
        )
        inside, so_far = (start, start)
        for k in reversed(range(count)) if reverse else range(count):
            passed = k > here if reverse else k < here
            so_far = combine(
                so_far, jax.tree.map(lambda part, own: part[k].astype(own.dtype), pieces, x)
            )
            inside = jax.tree.map(lambda new, old: jnp.where(passed, new, old), so_far, inside)
        before = combine(inside, before)
    return before


def gather_axes(x, axes, dim):
    filled = x
    for number in range(len(axes) - 1, -1, -1):
        filled = lax.all_gather(filled, axes[number], axis=dim, tiled=True)
    return filled


def prefix_matrix(length):
    row_index = lax.broadcasted_iota(jnp.int32, (length, length), 0)
    column_index = lax.broadcasted_iota(jnp.int32, (length, length), 1)
    return (column_index <= row_index).astype(jnp.float32)


def carry_combine(first_part, second_part):
    return (
        first_part[0] + second_part[0],
        jnp.exp(second_part[0])[..., None, None] * first_part[1] + second_part[1],
    )


def local_chain(states, totals, reverse):

    def advance(carried, operands):
        block_state, block_total = operands
        return (jnp.exp(block_total)[..., None, None] * carried + block_state, carried)

    start_state = jnp.zeros(states.shape[1:], jnp.float32)
    return lax.scan(advance, start_state, (states, totals), reverse=reverse)


def mix_tokens(
    value_projected,
    key_projected,
    query_projected,
    output_gate_projected,
    step_projected_raw,
    head_decay_logarithm,
    position_extra_decay,
    value_filter_weight,
    key_filter_weight,
    query_filter_weight,
    head_norm_gain,
):
    tokens = value_projected.shape[0]
    value_width = value_projected.shape[1]
    key_width = key_projected.shape[1]
    head_count = step_projected_raw.shape[2]
    group_count = key_width // STATE
    per_group = head_count // group_count
    blocks = tokens // BLOCK
    joined = jnp.concatenate([value_projected, key_projected, query_projected], axis=1)
    padded = padded_2(joined, ((SP, 0),), (TAPS - 1) // 2).astype(jnp.float32)
    weights = jnp.concatenate(
        [value_filter_weight, key_filter_weight, query_filter_weight], axis=1
    ).astype(jnp.float32)
    filtered = weights[0] * padded[0:tokens]
    for offset in range(1, TAPS):
        filtered = filtered + weights[offset] * padded[offset : offset + tokens]
    values = filtered[:, :value_width].astype(jnp.bfloat16)
    key_rows = jax.nn.silu(filtered[:, value_width : value_width + key_width]).astype(jnp.bfloat16)
    key_rows = key_rows.reshape(blocks, BLOCK, group_count, STATE)
    query_rows = jax.nn.silu(filtered[:, value_width + key_width :]).astype(jnp.bfloat16)
    query_rows = query_rows.reshape(blocks, BLOCK, group_count, STATE)
    positive_step_sizes = jax.nn.softplus(step_projected_raw.astype(jnp.float32))
    decay_logarithm = (
        -jnp.exp(head_decay_logarithm)[:, None, :] * positive_step_sizes
        + position_extra_decay[None]
    )
    scaled = (
        values.astype(jnp.float32).reshape(tokens, head_count, HEAD_DIM)[None]
        * positive_step_sizes[..., None]
    ).astype(jnp.bfloat16)
    scaled = scaled.reshape(2, blocks, BLOCK, group_count, per_group, HEAD_DIM)
    log_blocks = decay_logarithm.reshape(2, blocks, BLOCK, group_count, per_group)
    running = jnp.einsum("ls,dbsgh->dblgh", prefix_matrix(BLOCK), log_blocks)
    forward_cum = running[0]
    backward_excl = running[1] - log_blocks[1]
    forward_total = running[0][:, -1]
    backward_total = running[1][:, -1]
    scores = jnp.einsum("blgn,bsgn->blsg", query_rows, key_rows, preferred_element_type=jnp.float32)
    position = lax.broadcasted_iota(jnp.int32, (BLOCK,), 0)
    lower_mask = (position[None, :] <= position[:, None])[None, :, :, None, None]
    upper_mask = (position[None, :] >= position[:, None])[None, :, :, None, None]
    forward_gap = jnp.where(lower_mask, forward_cum[:, :, None] - forward_cum[:, None, :], -jnp.inf)
    backward_gap = jnp.where(
        upper_mask, backward_excl[:, None, :] - backward_excl[:, :, None], -jnp.inf
    )
    forward_weight = (scores[..., None] * jnp.exp(forward_gap)).astype(jnp.bfloat16)
    backward_weight = (scores[..., None] * jnp.exp(backward_gap)).astype(jnp.bfloat16)
    inner = jnp.einsum(
        "blsgh,bsghp->blghp", forward_weight, scaled[0], preferred_element_type=jnp.float32
    )
    inner = inner + jnp.einsum(
        "blsgh,bsghp->blghp", backward_weight, scaled[1], preferred_element_type=jnp.float32
    )
    key_wide = key_rows.astype(jnp.float32)[:, :, :, None, :]
    forward_keys = (jnp.exp(forward_total[:, None] - forward_cum)[..., None] * key_wide).astype(
        jnp.bfloat16
    )
    backward_keys = (jnp.exp(backward_excl)[..., None] * key_wide).astype(jnp.bfloat16)
    forward_state = jnp.einsum(
        "bsghn,bsghp->bghpn", forward_keys, scaled[0], preferred_element_type=jnp.float32
    )
    backward_state = jnp.einsum(
        "bsghn,bsghp->bghpn", backward_keys, scaled[1], preferred_element_type=jnp.float32
    )
    forward_final, forward_before = local_chain(forward_state, forward_total, False)
    backward_final, backward_before = local_chain(backward_state, backward_total, True)
    forward_sum = jnp.sum(forward_total, axis=0)
    backward_sum = jnp.sum(backward_total, axis=0)
    zero_total = jnp.zeros(forward_sum.shape, jnp.float32)
    zero_state = jnp.zeros(forward_final.shape, jnp.float32)
    entering = carried_in(
        (forward_sum, forward_final), SP, carry_combine, (zero_total, zero_state), False
    )[1]
    leaving = carried_in(
        (backward_sum, backward_final), SP, carry_combine, (zero_total, zero_state), True
    )[1]
    forward_prior = jnp.cumsum(forward_total, axis=0) - forward_total
    backward_after = backward_sum[None] - jnp.cumsum(backward_total, axis=0)
    forward_in = jnp.exp(forward_prior)[..., None, None] * entering[None] + forward_before
    backward_in = jnp.exp(backward_after)[..., None, None] * leaving[None] + backward_before
    forward_read = jnp.exp(forward_cum)[..., None] * jnp.einsum(
        "blgn,bghpn->blghp",
        query_rows,
        forward_in.astype(jnp.bfloat16),
        preferred_element_type=jnp.float32,
    )
    backward_read = jnp.exp(backward_total[:, None] - backward_excl)[..., None] * jnp.einsum(
        "blgn,bghpn->blghp",
        query_rows,
        backward_in.astype(jnp.bfloat16),
        preferred_element_type=jnp.float32,
    )
    mixer_raw = (inner + forward_read + backward_read).reshape(tokens, head_count, HEAD_DIM)
    gated = mixer_raw * jax.nn.silu(output_gate_projected.astype(jnp.float32)).reshape(
        tokens, head_count, HEAD_DIM
    )
    inverse_rms = lax.rsqrt(jnp.mean(gated * gated, axis=-1, keepdims=True) + epsilon)
    head_normed = (gated * inverse_rms * head_norm_gain.reshape(head_count, HEAD_DIM)).astype(
        jnp.bfloat16
    )
    return head_normed.reshape(tokens, head_count * HEAD_DIM)


def slot_table(route_rows, experts, capacity):
    flat_ids = route_rows.reshape(-1)
    expert_ids = lax.broadcasted_iota(jnp.int32, (flat_ids.shape[0], experts), 1)
    matches = (flat_ids[:, None] == expert_ids).astype(jnp.int32)
    earlier = jnp.cumsum(matches, axis=0) - matches
    rank_in = jnp.sum(matches * earlier, axis=1)
    return (flat_ids * capacity + rank_in).reshape(route_rows.shape)


def dispatch_rows(slots, token_rows, places):
    place_ids = lax.broadcasted_iota(jnp.int32, (places,) + slots.shape, 0)
    one_hot = jnp.sum((place_ids == slots[None]).astype(jnp.float32), axis=2).astype(jnp.bfloat16)
    return jnp.dot(one_hot, token_rows, preferred_element_type=jnp.float32).astype(jnp.bfloat16)


def shards(
    residual_layer_input,
    value_projected,
    key_projected,
    query_projected,
    output_gate_projected,
    step_projected_raw,
    head_decay_logarithm,
    position_extra_decay,
    value_filter_weight,
    key_filter_weight,
    query_filter_weight,
    head_norm_gain,
    mixer_output_matrix,
    expert_norm_gain,
    routes,
    chosen_expert_weight,
    expert_gate_matrix,
    expert_up_matrix,
    expert_down_matrix,
):
    heads_out = mix_tokens(
        value_projected,
        key_projected,
        query_projected,
        output_gate_projected,
        step_projected_raw,
        head_decay_logarithm,
        position_extra_decay,
        value_filter_weight,
        key_filter_weight,
        query_filter_weight,
        head_norm_gain,
    )
    projected = jnp.dot(
        gather_axes(heads_out, TP, 1), mixer_output_matrix, preferred_element_type=jnp.float32
    ).astype(jnp.bfloat16)
    mixer_out = lax.all_to_all(projected, TP, split_axis=0, concat_axis=1, tiled=True)
    middle = (residual_layer_input.astype(jnp.float32) + mixer_out.astype(jnp.float32)).astype(
        jnp.bfloat16
    )
    residual = middle.astype(jnp.float32)
    normed = (
        residual
        * lax.rsqrt(jnp.mean(residual * residual, axis=-1, keepdims=True) + epsilon)
        * expert_norm_gain
    ).astype(jnp.bfloat16)
    own_rows = normed.shape[0]
    model_width = normed.shape[1]
    top_count = routes.shape[1]
    experts = lax.axis_size(SP)
    capacity = 2 * own_rows * top_count // experts
    places = experts * capacity
    position = lax.axis_index(TP)
    own_routes = lax.dynamic_slice_in_dim(routes, position * own_rows, own_rows, 0)
    own_slots = slot_table(own_routes, experts, capacity)
    outgoing = dispatch_rows(own_slots, normed, places)
    received = lax.all_to_all(
        outgoing.reshape(experts, capacity, model_width),
        SP,
        split_axis=0,
        concat_axis=0,
        tiled=True,
    )
    arrived = lax.all_gather(received[None], TP, axis=0, tiled=True)
    slot_rows = arrived.reshape(-1, model_width)
    gate_value = jnp.dot(slot_rows, expert_gate_matrix[0], preferred_element_type=jnp.float32)
    up_value = jnp.dot(slot_rows, expert_up_matrix[0], preferred_element_type=jnp.float32)
    hidden = (jax.nn.silu(gate_value) * up_value).astype(jnp.bfloat16)
    partial_sum = jnp.dot(hidden, expert_down_matrix[0], preferred_element_type=jnp.float32).astype(
        jnp.bfloat16
    )
    summed = lax.psum_scatter(
        partial_sum.astype(jnp.float32).reshape(arrived.shape).astype(jnp.bfloat16),
        TP,
        scatter_dimension=0,
        tiled=True,
    )
    results = summed.reshape(experts, capacity, model_width)
    returned = lax.all_to_all(results, SP, split_axis=0, concat_axis=0, tiled=True)
    chosen = (
        lax.broadcasted_iota(jnp.int32, (own_rows, top_count, places), 2) == own_slots[:, :, None]
    )
    mixing = jnp.sum(jnp.where(chosen, chosen_expert_weight[:, :, None], 0.0), axis=1)
    expert_mix = jnp.dot(mixing, returned.reshape(places, model_width).astype(jnp.float32))
    return (residual + expert_mix).astype(jnp.bfloat16)


def solution(mesh):
    finer = Mesh(mesh.devices.reshape(8, 4, 8, 2), ("sp_0", "sp_1", "tp_0", "tp_1"))
    return jax.shard_map(
        shards,
        mesh=finer,
        in_specs=(
            P(SP_TP, None),
            P(SP, TP),
            P(SP, TP),
            P(SP, TP),
            P(SP, TP),
            P(None, SP, TP),
            P(None, TP),
            P(SP, TP),
            P(None, TP),
            P(None, TP),
            P(None, TP),
            P(TP),
            P(None, TP),
            P(),
            P(SP, None),
            P(SP_TP, None),
            P(SP, None, TP),
            P(SP, None, TP),
            P(SP, TP, None),
        ),
        out_specs=P(SP_TP, None),
        check_vma=False,
    )
```

profile of v0, /device:TPU:25, one launch (start us, length us, event | category | flops | bytes accessed | tf_op | source)
XLA Modules:
  0.0 411.3 jit_solution(13802664168214537956)
XLA Ops:
  6.5 1.1 copy.131
  9.7 3.1 collective-permute-start
  12.8 1.3 collective-permute-start.1
  17.8 1.3 dynamic-slice
  20.2 9.9 %all-reduce.2 = (bf16[16]{0:T(256)(128)(2,1)S(1)}, bf16[16]{0:T(256)(128)(2,1)S(1)}) all-reduce(bf16[16]{0:T(256)(128)(2,1)S(1)} %dynamic-update-slice.1, bf16[16]{0:T(256)(128)(2,1)S(1)} %dynamic-update-slice), channel_id=4, replica_groups=mesh['sp_0'=8,'sp_1'=4,'tp_0'=8,'tp_1'=2] {'sp_1'}, use_global_device_ids=true, to_apply=%add.1 | all-reduce | flops 32 | bytes 128
  30.1 18.0 %all_gather.46 = bf16[8,1,4]{2,1,0:T(2,128)(2,1)S(1)} all-gather(bf16[1,1,4]{2,1,0:T(2,128)(2,1)S(1)} %get-tuple-element.265), channel_id=1, replica_groups=mesh['sp_0'=8,'sp_1'=4,'tp_0'=8,'tp_1'=2] {'sp_0'}, dimensions={0}, use_global_device_ids=true | all-gather | bytes 72 | tf_op jit(solution)/shard_map/all_gather | solution.py:46
  48.8 9.8 %all_gather.51 = bf16[8,1,4]{2,1,0:T(2,128)(2,1)S(1)} all-gather(bf16[1,1,4]{2,1,0:T(2,128)(2,1)S(1)} %get-tuple-element.269), channel_id=1, replica_groups=mesh['sp_0'=8,'sp_1'=4,'tp_0'=8,'tp_1'=2] {'sp_0'}, dimensions={0}, use_global_device_ids=true | all-gather | bytes 72 | tf_op jit(solution)/shard_map/all_gather | solution.py:46
  67.6 9.4 %all-gather.1 = bf16[4,4,64,128]{3,2,1,0:T(8,128)(2,1)S(1)} all-gather(bf16[1,4,64,128]{3,2,1,0:T(8,128)(2,1)S(1)} %convert_element_type.652), channel_id=3, replica_groups=mesh['sp_0'=8,'sp_1'=4,'tp_0'=8,'tp_1'=2] {'sp_1'}, dimensions={0}, use_global_device_ids=true | all-gather | bytes 327680 | tf_op jit(solution)/shard_map/all_gather | solution.py:46
  77.1 19.1 %all_gather.49 = bf16[8,1,4,64,128]{4,3,2,1,0:T(8,128)(2,1)S(1)} all-gather(bf16[1,1,4,64,128]{4,3,2,1,0:T(8,128)(2,1)S(1)} %fusion.75), channel_id=1, replica_groups=mesh['sp_0'=8,'sp_1'=4,'tp_0'=8,'tp_1'=2] {'sp_0'}, dimensions={0}, use_global_device_ids=true | all-gather | bytes 589824 | tf_op jit(solution)/shard_map/all_gather | solution.py:46
  96.6 1.5 while.31
  98.2 9.7 %all-gather.3 = bf16[4,4,64,128]{3,2,1,0:T(8,128)(2,1)S(1)} all-gather(bf16[1,4,64,128]{3,2,1,0:T(8,128)(2,1)S(1)} %convert_element_type.683), channel_id=5, replica_groups=mesh['sp_0'=8,'sp_1'=4,'tp_0'=8,'tp_1'=2] {'sp_1'}, dimensions={0}, use_global_device_ids=true | all-gather | bytes 327680 | tf_op jit(solution)/shard_map/all_gather | solution.py:46
  108.0 19.3 %all_gather.54 = bf16[8,1,4,64,128]{4,3,2,1,0:T(8,128)(2,1)S(1)} all-gather(bf16[1,1,4,64,128]{4,3,2,1,0:T(8,128)(2,1)S(1)} %fusion.72), channel_id=1, replica_groups=mesh['sp_0'=8,'sp_1'=4,'tp_0'=8,'tp_1'=2] {'sp_0'}, dimensions={0}, use_global_device_ids=true | all-gather | bytes 589824 | tf_op jit(solution)/shard_map/all_gather | solution.py:46
  129.0 1.3 fusion.29
  130.3 1.3 fusion.6
  131.7 1.1 fusion.63
  134.8 1.2 fusion.34
  137.0 30.0 %all_gather.55 = bf16[256,512]{0,1:T(8,128)(2,1)} all-gather(bf16[256,256]{0,1:T(8,128)(2,1)S(1)} %fusion.32), channel_id=1, replica_groups=mesh['sp_0'=8,'sp_1'=4,'tp_0'=8,'tp_1'=2] {'tp_1'}, dimensions={1}, use_global_device_ids=true | all-gather | bytes 393216 | tf_op jit(solution)/shard_map/all_gather | solution.py:64
  168.4 33.5 %all-gather.8.cloned.1.call-done = bf16[256,4096]{0,1:T(8,128)(2,1)} async-done(((bf16[256,512]{0,1:T(8,128)(2,1)}), bf16[256,4096]{0,1:T(8,128)(2,1)}) %all-gather.8.cloned.1.call-update) | async-done | bytes 2097168 | tf_op jit(solution)/shard_map/all_gather | solution.py:64
  201.9 3.2 convolution_convert_fusion.2
  205.1 10.1 %all-to-all-start = ((bf16[16,16,128]{2,1,0:T(8,128)(2,1)}), bf16[16,16,128]{2,1,0:T(8,128)(2,1)S(1)}, u32[]{:S(2)}, u32[]{:S(2)}) async-start(bf16[16,16,128]{2,1,0:T(8,128)(2,1)} %bitcast.67), calls=%async_computation | async-start | bytes 131072 | tf_op jit(solution)/shard_map/all_to_all | solution.py:258
  215.4 4.7 %all-to-all-done = bf16[16,16,128]{2,1,0:T(8,128)(2,1)S(1)} async-done(((bf16[16,16,128]{2,1,0:T(8,128)(2,1)}), bf16[16,16,128]{2,1,0:T(8,128)(2,1)S(1)}, u32[]{:S(2)}, u32[]{:S(2)}) %all-to-all-start) | async-done | bytes 65568 | tf_op jit(solution)/shard_map/all_to_all | solution.py:258
  220.8 21.4 %all_to_all.23 = bf16[32,2,2048]{2,1,0:T(2,128)(2,1)} all-to-all(bf16[32,2,2048]{2,1,0:T(2,128)(2,1)S(1)} %reshape.1011), channel_id=1, replica_groups=mesh['sp_0'=8,'sp_1'=4,'tp_0'=8,'tp_1'=2] {'sp_0','sp_1'}, dimensions={0} | all-to-all | bytes 524288 | tf_op jit(solution)/shard_map/all_to_all | solution.py:278
  242.4 38.9 %all-gather.10.cloned.1.call-done = bf16[512,2,2048]{2,1,0:T(2,128)(2,1)} async-done(((bf16[32,2,2048]{2,1,0:T(2,128)(2,1)}), bf16[512,2,2048]{2,1,0:T(2,128)(2,1)}) %all-gather.10.cloned.1.call-update) | async-done | bytes 4194320 | tf_op jit(solution)/shard_map/all_gather | solution.py:285
  281.3 7.2 %reshape.1012 = bf16[1024,2048]{1,0:T(8,128)(2,1)} reshape(bf16[512,2,2048]{2,1,0:T(2,128)(2,1)} %all-gather.10.cloned.1.call-done) | data formatting | bytes 8388608 | tf_op jit(solution)/shard_map/reshape | solution.py:286
  288.5 4.5 %fusion.14 = f32[1024,256]{1,0:T(8,128)} fusion(bf16[1024,2048]{1,0:T(8,128)(2,1)} %reshape.1012, bf16[1,2048,256]{2,1,0:T(8,128)(2,1)S(1)} %copy-done.16), kind=kOutput, calls=%fused_computation.31 | convolution fusion | flops 1073741824 | bytes 6291456 | tf_op jit(solution)/shard_map/dot_general | solution.py:287
  293.0 9.1 %convolution_convert_fusion = bf16[1024,2048]{1,0:T(8,128)(2,1)} fusion(bf16[1024,2048]{1,0:T(8,128)(2,1)} %reshape.1012, bf16[1,256,2048]{2,1,0:T(8,128)(2,1)S(1)} %copy-done, bf16[1,2048,256]{2,1,0:T(8,128)(2,1)} %param.40, f32[1024,256]{1,0:T(8,128)} %fusion.14), kind=kOutput, calls=%fused_computation.10 | convolution fusion | flops 2151153664 | bytes 11534336 | tf_op jit(solution)/shard_map/dot_general | solution.py:290
  302.1 7.6 %convert_element_type.713 = bf16[16,32,2,2048]{3,2,1,0:T(2,128)(2,1)} reshape(bf16[1024,2048]{1,0:T(8,128)(2,1)} %convolution_convert_fusion) | data formatting | bytes 8388608 | tf_op jit(solution)/shard_map/convert_element_type | solution.py:294
  309.8 6.1 %copy.156 = bf16[16,32,2,2048]{3,1,2,0:T(8,128)(2,1)} copy(bf16[16,32,2,2048]{3,2,1,0:T(2,128)(2,1)} %convert_element_type.713) | data formatting | bytes 8388608 | tf_op jit(solution)/shard_map/convert_element_type | solution.py:294
  315.8 64.9 %reduce-scatter.2.cloned.1.call-done = bf16[1,32,2,2048]{3,1,2,0:T(8,128)(2,1)} async-done(((bf16[16,32,2,2048]{3,1,2,0:T(8,128)(2,1)}), bf16[1,32,2,2048]{3,1,2,0:T(8,128)(2,1)}) %reduce-scatter.2.cloned.1.call-update) | async-done | bytes 262160 | tf_op jit(solution)/shard_map/reduce_scatter | solution.py:293
  380.8 1.9 copy.157
  382.7 10.1 %all-to-all-start.2 = ((bf16[32,2,2048]{2,1,0:T(2,128)(2,1)}), bf16[32,2,2048]{2,1,0:T(2,128)(2,1)S(1)}, u32[]{:S(2)}, u32[]{:S(2)}) async-start(bf16[32,2,2048]{2,1,0:T(2,128)(2,1)} %copy.157), calls=%async_computation.3 | async-start | bytes 524288 | tf_op jit(solution)/shard_map/all_to_all | solution.py:300
  392.8 11.1 %all-to-all-done.2 = bf16[32,2,2048]{2,1,0:T(2,128)(2,1)S(1)} async-done(((bf16[32,2,2048]{2,1,0:T(2,128)(2,1)}), bf16[32,2,2048]{2,1,0:T(2,128)(2,1)S(1)}, u32[]{:S(2)}, u32[]{:S(2)}) %all-to-all-start.2) | async-done | bytes 262176 | tf_op jit(solution)/shard_map/all_to_all | solution.py:300
  (134 shorter events, 26.0 us)
Async XLA Ops:
  6.5 286.5 %copy-start = (bf16[1,256,2048]{2,1,0:T(8,128)(2,1)S(1)}, bf16[1,256,2048]{2,1,0:T(8,128)(2,1)}, u32[]{:S(2)}) copy-start(bf16[1,256,2048]{2,1,0:T(8,128)(2,1)} %param.41) | copy-start | bytes 3145732
  6.5 195.4 %all-gather.8.cloned.1.call-start = ((), (), s32[]{:S(2)}) async-start(), calls=%async_computation.4 | async-start | bytes 2359296 | tf_op jit(solution)/shard_map/all_gather | solution.py:64
  9.7 54.5 %collective-permute-start = (bf16[2,512]{0,1:T(8,128)(2,1)S(1)}, bf16[2,512]{0,1:T(8,128)(2,1)S(1)}, u32[]{:S(2)}, u32[]{:S(2)}) collective-permute-start(bf16[2,512]{0,1:T(8,128)(2,1)S(1)} %get-tuple-element.275), channel_id=1, source_target_pairs={{0,16},{16,32},{32,48},{48,64},{64,80},{80,96},{96,112},{112,128},... | collective-permute-start | bytes 6152 | tf_op jit(solution)/shard_map/ppermute | solution.py:25
  12.8 51.4 %collective-permute-start.1 = (bf16[2,512]{0,1:T(8,128)(2,1)S(1)}, bf16[2,512]{0,1:T(8,128)(2,1)S(1)}, u32[]{:S(2)}, u32[]{:S(2)}) collective-permute-start(bf16[2,512]{0,1:T(8,128)(2,1)S(1)} %get-tuple-element.276), channel_id=1, source_target_pairs={{16,0},{32,16},{48,32},{64,48},{80,64},{96,80},{112,96},{128,112},... | collective-permute-start | bytes 6152 | tf_op jit(solution)/shard_map/ppermute | solution.py:27
  17.8 46.3 %copy-start.5 = (f32[2,4]{1,0:T(2,128)}, f32[2,4]{1,0:T(2,128)S(1)}, u32[]{:S(2)}) copy-start(f32[2,4]{1,0:T(2,128)S(1)} %get-tuple-element.240) | copy-start | bytes 100
  62.3 14.6 %copy-start.7 = (f32[4]{0:T(128)}, f32[4]{0:T(128)S(1)}, u32[]{:S(2)}) copy-start(f32[4]{0:T(128)S(1)} %get-tuple-element.308) | copy-start | bytes 52
  62.3 14.6 %copy-start.8 = (f32[4]{0:T(128)}, f32[4]{0:T(128)S(1)}, u32[]{:S(2)}) copy-start(f32[4]{0:T(128)S(1)} %get-tuple-element.309) | copy-start | bytes 52
  62.3 14.6 %copy-start.9 = (f32[4]{0:T(128)}, f32[4]{0:T(128)S(1)}, u32[]{:S(2)}) copy-start(f32[4]{0:T(128)S(1)} %get-tuple-element.310) | copy-start | bytes 52
  62.3 14.6 %copy-start.10 = (f32[4]{0:T(128)}, f32[4]{0:T(128)S(1)}, u32[]{:S(2)}) copy-start(f32[4]{0:T(128)S(1)} %get-tuple-element.311) | copy-start | bytes 52
  66.5 0.6 copy-start.2
  67.2 40.6 %copy-start.11 = (f32[4]{0:T(128)S(1)}, f32[4]{0:T(128)}, u32[]{:S(2)}) copy-start(f32[4]{0:T(128)} %get-tuple-element.313) | copy-start | bytes 52
  67.2 40.6 %copy-start.12 = (f32[4]{0:T(128)S(1)}, f32[4]{0:T(128)}, u32[]{:S(2)}) copy-start(f32[4]{0:T(128)} %get-tuple-element.314) | copy-start | bytes 52
  67.2 40.6 %copy-start.13 = (f32[4]{0:T(128)S(1)}, f32[4]{0:T(128)}, u32[]{:S(2)}) copy-start(f32[4]{0:T(128)} %get-tuple-element.315) | copy-start | bytes 52
  67.2 40.6 %copy-start.14 = (f32[4]{0:T(128)S(1)}, f32[4]{0:T(128)}, u32[]{:S(2)}) copy-start(f32[4]{0:T(128)} %get-tuple-element.316) | copy-start | bytes 52
  67.5 29.1 %copy-start.1 = (f32[2,1,4,64,128]{4,3,2,1,0:T(8,128)}, f32[2,1,4,64,128]{4,3,2,1,0:T(8,128)S(1)}, u32[]{:S(2)}) copy-start(f32[2,1,4,64,128]{4,3,2,1,0:T(8,128)S(1)} %get-tuple-element.138) | copy-start | bytes 786436
  96.2 11.6 %copy-start.3 = (bf16[2,128,4,64]{1,0,3,2:T(2,128)(2,1)}, bf16[2,128,4,64]{1,0,3,2:T(2,128)(2,1)S(1)}, u32[]{:S(2)}) copy-start(bf16[2,128,4,64]{1,0,3,2:T(2,128)(2,1)S(1)} %reshape.1006) | copy-start | bytes 393220
  132.7 87.4 %copy-start.4 = (bf16[16,2048]{1,0:T(8,128)(2,1)S(1)}, bf16[16,2048]{1,0:T(8,128)(2,1)}, u32[]{:S(2)}) copy-start(bf16[16,2048]{1,0:T(8,128)(2,1)} %param.23) | copy-start | bytes 196612
  132.8 87.5 %copy-start.6 = (f32[2048]{0:T(1024)S(1)}, f32[2048]{0:T(1024)}, u32[]{:S(2)}) copy-start(f32[2048]{0:T(1024)} %param.36) | copy-start | bytes 24580
  205.1 15.0 %all-to-all-start = ((bf16[16,16,128]{2,1,0:T(8,128)(2,1)}), bf16[16,16,128]{2,1,0:T(8,128)(2,1)S(1)}, u32[]{:S(2)}, u32[]{:S(2)}) async-start(bf16[16,16,128]{2,1,0:T(8,128)(2,1)} %bitcast.67), calls=%async_computation | async-start | bytes 131072 | tf_op jit(solution)/shard_map/all_to_all | solution.py:258
  215.2 66.2 %all-gather.10.cloned.1.call-start = ((), (), s32[]{:S(2)}) async-start(), calls=%async_computation.6 | async-start | bytes 4456448 | tf_op jit(solution)/shard_map/all_gather | solution.py:285
  242.2 46.4 %copy-start.16 = (bf16[1,2048,256]{2,1,0:T(8,128)(2,1)S(1)}, bf16[1,2048,256]{2,1,0:T(8,128)(2,1)}, u32[]{:S(2)}) copy-start(bf16[1,2048,256]{2,1,0:T(8,128)(2,1)} %param.39) | copy-start | bytes 3145732
  242.2 138.6 %reduce-scatter.2.cloned.1.call-start = ((), (), s32[]{:S(2)}) async-start(), calls=%async_computation.5 | async-start | bytes 4456448 | tf_op jit(solution)/shard_map/reduce_scatter | solution.py:293
  315.8 76.9 %copy-start.15 = (f32[16,2]{0,1:T(2,128)S(1)}, f32[16,2]{0,1:T(2,128)}, u32[]{:S(2)}) copy-start(f32[16,2]{0,1:T(2,128)} %param.38) | copy-start | bytes 388
  382.7 21.2 %all-to-all-start.2 = ((bf16[32,2,2048]{2,1,0:T(2,128)(2,1)}), bf16[32,2,2048]{2,1,0:T(2,128)(2,1)S(1)}, u32[]{:S(2)}, u32[]{:S(2)}) async-start(bf16[32,2,2048]{2,1,0:T(2,128)(2,1)} %copy.157), calls=%async_computation.3 | async-start | bytes 524288 | tf_op jit(solution)/shard_map/all_to_all | solution.py:300
Sparse Core Ops, SparseCore 0:
  167.2 34.6 all-gather.7
  242.3 39.0 all-gather.9
  316.0 64.7 reduce-scatter.1
where the time goes:
time: 413 us; the launch traced here: 411 us
  waiting for transfers between devices  153 us (37%)
  blocking collectives  147 us (36%)
  local copies, waits for them, and re-layouts  35.1 us (8%)
  starting transfers between devices  24.8 us (6%)
  matrix products  23.8 us (6%)
  between operations  14.4 us (3%)
  other arithmetic  13.5 us (3%)
    all_gather x6, blocking collectives, carried_in(): lax.all_gather(part.astype(kind), axis)  85.3 us
    reduce_scatter x1, waiting for transfers between devices, shards(): lax.psum_scatter(partial_sum.astype(jnp.float32).reshape(arrived.shape).a...  64.9 us
    all_gather x1, waiting for transfers between devices, shards(): arrived = lax.all_gather(received[None], TP, axis=0, tiled=True)  38.9 us
    all_gather x1, waiting for transfers between devices, gather_axes(): filled = lax.all_gather(filled, axes[number], axis=dim, tiled=True)  33.5 us
    all_gather x1, blocking collectives, gather_axes(): filled = lax.all_gather(filled, axes[number], axis=dim, tiled=True)  30 us
    all_to_all x1, blocking collectives, shards(): lax.all_to_all(outgoing.reshape(experts, capacity, model_width), SP, spli...  21.4 us
    convert_element_type x2, local copies, waits for them, and re-layouts, shards(): partial_sum.astype(jnp.float32).reshape(arrived.shape).astype(jnp.bfloat16)  13.7 us
    all_to_all x1, waiting for transfers between devices, shards(): lax.all_to_all(results, SP, split_axis=0, concat_axis=0, tiled=True)  11.1 us
  transfers between devices with their start and end apart: 7, of which 5 were waited for; matrix products, arithmetic and copies ran while one was open for 3% of the time, Pallas kernels for 0%

commit v1 on v0

--- a/solution.py
+++ b/solution.py
@@ -12,6 +12,13 @@
 TP = ("tp_0", "tp_1")
 SP_TP = ("sp_0", "sp_1", "tp_0", "tp_1")
 epsilon = 1e-06
+
+
+def exchange_gather(x, mesh_axis, dim):
+    size = lax.axis_size(mesh_axis)
+    blocks = jnp.stack([x for _ in range(size)])
+    blocks = lax.all_to_all(blocks, mesh_axis, split_axis=0, concat_axis=0)
+    return jnp.concatenate(blocks, axis=dim)
 
 
 def padded_2(cells, sides, width):
@@ -282,7 +289,7 @@
         concat_axis=0,
         tiled=True,
     )
-    arrived = lax.all_gather(received[None], TP, axis=0, tiled=True)
+    arrived = exchange_gather(received[None], TP, 0)
     slot_rows = arrived.reshape(-1, model_width)
     gate_value = jnp.dot(slot_rows, expert_gate_matrix[0], preferred_element_type=jnp.float32)
     up_value = jnp.dot(slot_rows, expert_up_matrix[0], preferred_element_type=jnp.float32)

time: 413 us -> 473 us (1.15)
  blocking collectives: 147 us -> 249 us
  waiting for transfers between devices: 153 us -> 108 us
    all_to_all x0 -> x1, blocking collectives: none -> 102 us  [exchange_gather(): blocks = lax.all_to_all(blocks, mesh_axis, split_axis=0, concat_axis=0)]
    all_gather x1 -> x0, waiting for transfers between devices: 38.9 us -> none  [shards(): arrived = lax.all_gather(received[None], TP, axis=0, tiled=True)]
    another operation x7 -> x9, local copies, waits for them, and re-layouts: 1.74 us -> 12.2 us  [the longest x1 7.27 us: shards(): slot_rows = arrived.reshape(-1, model_width)]
    reshape x1 -> x0, local copies, waits for them, and re-layouts: 7.19 us -> none  [shards(): slot_rows = arrived.reshape(-1, model_width)]
    reduce_scatter x1, waiting for transfers between devices: 64.9 us -> 58.6 us  [shards(): lax.psum_scatter(partial_sum.astype(jnp.float32).reshape(arrived.shape).a...]
  transfers between devices with their start and end apart: 7 -> 6, of which waited for: 5 -> 4; matrix products, arithmetic and copies ran while one was open for 3% -> 3% of each run, Pallas kernels for 0% -> 0%
where the time goes in v1:
time: 473 us; the launch traced here: 471 us
  blocking collectives  249 us (53%)
  waiting for transfers between devices  108 us (23%)
  local copies, waits for them, and re-layouts  38.4 us (8%)
  starting transfers between devices  24.4 us (5%)
  matrix products  23.8 us (5%)
  between operations  14.7 us (3%)
  other arithmetic  13.4 us (3%)
    all_to_all x1, blocking collectives, exchange_gather(): blocks = lax.all_to_all(blocks, mesh_axis, split_axis=0, concat_axis=0)  102 us
    all_gather x6, blocking collectives, carried_in(): lax.all_gather(part.astype(kind), axis)  85.2 us
    reduce_scatter x1, waiting for transfers between devices, shards(): lax.psum_scatter(partial_sum.astype(jnp.float32).reshape(arrived.shape).a...  58.6 us
    all_gather x1, waiting for transfers between devices, gather_axes(): filled = lax.all_gather(filled, axes[number], axis=dim, tiled=True)  33.5 us
    all_gather x1, blocking collectives, gather_axes(): filled = lax.all_gather(filled, axes[number], axis=dim, tiled=True)  30.1 us
    all_to_all x1, blocking collectives, shards(): lax.all_to_all(outgoing.reshape(experts, capacity, model_width), SP, spli...  21.3 us
    convert_element_type x2, local copies, waits for them, and re-layouts, shards(): partial_sum.astype(jnp.float32).reshape(arrived.shape).astype(jnp.bfloat16)  13.7 us
    all_to_all x1, waiting for transfers between devices, shards(): lax.all_to_all(results, SP, split_axis=0, concat_axis=0, tiled=True)  11.1 us
  transfers between devices with their start and end apart: 6, of which 4 were waited for; matrix products, arithmetic and copies ran while one was open for 3% of the time, Pallas kernels for 0%

profile of v1, /device:TPU:25, one launch (start us, length us, event | category | flops | bytes accessed | tf_op | source)
XLA Modules:
  0.0 471.4 jit_solution(9273919303022134508)
XLA Ops:
  6.5 1.1 copy.131
  9.7 3.1 collective-permute-start
  12.8 1.3 collective-permute-start.1
  17.8 1.3 dynamic-slice
  20.2 9.9 %all-reduce.2 = (bf16[16]{0:T(256)(128)(2,1)S(1)}, bf16[16]{0:T(256)(128)(2,1)S(1)}) all-reduce(bf16[16]{0:T(256)(128)(2,1)S(1)} %dynamic-update-slice.1, bf16[16]{0:T(256)(128)(2,1)S(1)} %dynamic-update-slice), channel_id=4, replica_groups=mesh['sp_0'=8,'sp_1'=4,'tp_0'=8,'tp_1'=2] {'sp_1'}, use_global_device_ids=true, to_apply=%add.1 | all-reduce | flops 32 | bytes 128
  30.1 18.0 %all_gather.43 = bf16[8,1,4]{2,1,0:T(2,128)(2,1)S(1)} all-gather(bf16[1,1,4]{2,1,0:T(2,128)(2,1)S(1)} %get-tuple-element.265), channel_id=1, replica_groups=mesh['sp_0'=8,'sp_1'=4,'tp_0'=8,'tp_1'=2] {'sp_0'}, dimensions={0}, use_global_device_ids=true | all-gather | bytes 72 | tf_op jit(solution)/shard_map/all_gather | solution.py:53
  48.8 9.8 %all_gather.48 = bf16[8,1,4]{2,1,0:T(2,128)(2,1)S(1)} all-gather(bf16[1,1,4]{2,1,0:T(2,128)(2,1)S(1)} %get-tuple-element.269), channel_id=1, replica_groups=mesh['sp_0'=8,'sp_1'=4,'tp_0'=8,'tp_1'=2] {'sp_0'}, dimensions={0}, use_global_device_ids=true | all-gather | bytes 72 | tf_op jit(solution)/shard_map/all_gather | solution.py:53
  67.6 9.4 %all-gather.1 = bf16[4,4,64,128]{3,2,1,0:T(8,128)(2,1)S(1)} all-gather(bf16[1,4,64,128]{3,2,1,0:T(8,128)(2,1)S(1)} %convert_element_type.652), channel_id=3, replica_groups=mesh['sp_0'=8,'sp_1'=4,'tp_0'=8,'tp_1'=2] {'sp_1'}, dimensions={0}, use_global_device_ids=true | all-gather | bytes 327680 | tf_op jit(solution)/shard_map/all_gather | solution.py:53
  77.1 19.1 %all_gather.46 = bf16[8,1,4,64,128]{4,3,2,1,0:T(8,128)(2,1)S(1)} all-gather(bf16[1,1,4,64,128]{4,3,2,1,0:T(8,128)(2,1)S(1)} %fusion.75), channel_id=1, replica_groups=mesh['sp_0'=8,'sp_1'=4,'tp_0'=8,'tp_1'=2] {'sp_0'}, dimensions={0}, use_global_device_ids=true | all-gather | bytes 589824 | tf_op jit(solution)/shard_map/all_gather | solution.py:53
  96.6 1.6 while.31
  98.2 9.7 %all-gather.3 = bf16[4,4,64,128]{3,2,1,0:T(8,128)(2,1)S(1)} all-gather(bf16[1,4,64,128]{3,2,1,0:T(8,128)(2,1)S(1)} %convert_element_type.683), channel_id=5, replica_groups=mesh['sp_0'=8,'sp_1'=4,'tp_0'=8,'tp_1'=2] {'sp_1'}, dimensions={0}, use_global_device_ids=true | all-gather | bytes 327680 | tf_op jit(solution)/shard_map/all_gather | solution.py:53
  108.0 19.3 %all_gather.51 = bf16[8,1,4,64,128]{4,3,2,1,0:T(8,128)(2,1)S(1)} all-gather(bf16[1,1,4,64,128]{4,3,2,1,0:T(8,128)(2,1)S(1)} %fusion.72), channel_id=1, replica_groups=mesh['sp_0'=8,'sp_1'=4,'tp_0'=8,'tp_1'=2] {'sp_0'}, dimensions={0}, use_global_device_ids=true | all-gather | bytes 589824 | tf_op jit(solution)/shard_map/all_gather | solution.py:53
  129.0 1.3 fusion.29
  130.3 1.3 fusion.6
  134.8 1.2 fusion.34
  137.0 30.1 %all_gather.52 = bf16[256,512]{0,1:T(8,128)(2,1)} all-gather(bf16[256,256]{0,1:T(8,128)(2,1)S(1)} %fusion.32), channel_id=1, replica_groups=mesh['sp_0'=8,'sp_1'=4,'tp_0'=8,'tp_1'=2] {'tp_1'}, dimensions={1}, use_global_device_ids=true | all-gather | bytes 393216 | tf_op jit(solution)/shard_map/all_gather | solution.py:71
  168.5 33.5 %all-gather.6.cloned.1.call-done = bf16[256,4096]{0,1:T(8,128)(2,1)} async-done(((bf16[256,512]{0,1:T(8,128)(2,1)}), bf16[256,4096]{0,1:T(8,128)(2,1)}) %all-gather.6.cloned.1.call-update) | async-done | bytes 2097168 | tf_op jit(solution)/shard_map/all_gather | solution.py:71
  201.9 3.2 convolution_convert_fusion.2
  205.2 10.1 %all-to-all-start = ((bf16[16,16,128]{2,1,0:T(8,128)(2,1)}), bf16[16,16,128]{2,1,0:T(8,128)(2,1)S(1)}, u32[]{:S(2)}, u32[]{:S(2)}) async-start(bf16[16,16,128]{2,1,0:T(8,128)(2,1)} %bitcast.67), calls=%async_computation | async-start | bytes 131072 | tf_op jit(solution)/shard_map/all_to_all | solution.py:265
  215.4 4.7 %all-to-all-done = bf16[16,16,128]{2,1,0:T(8,128)(2,1)S(1)} async-done(((bf16[16,16,128]{2,1,0:T(8,128)(2,1)}), bf16[16,16,128]{2,1,0:T(8,128)(2,1)S(1)}, u32[]{:S(2)}, u32[]{:S(2)}) %all-to-all-start) | async-done | bytes 65568 | tf_op jit(solution)/shard_map/all_to_all | solution.py:265
  220.8 21.3 %all_to_all.28 = bf16[32,2,2048]{2,1,0:T(2,128)(2,1)S(1)} all-to-all(bf16[32,2,2048]{2,1,0:T(2,128)(2,1)S(1)} %reshape.1010), channel_id=1, replica_groups=mesh['sp_0'=8,'sp_1'=4,'tp_0'=8,'tp_1'=2] {'sp_0','sp_1'}, dimensions={0} | all-to-all | bytes 524288 | tf_op jit(solution)/shard_map/all_to_all | solution.py:285
  242.1 3.2 stack.3
  245.3 102.1 %all_to_all.29 = bf16[16,1,32,2,2048]{4,3,2,1,0:T(2,128)(2,1)} all-to-all(bf16[16,1,32,2,2048]{4,3,2,1,0:T(2,128)(2,1)S(1)} %stack.3), channel_id=1, replica_groups=mesh['sp_0'=8,'sp_1'=4,'tp_0'=8,'tp_1'=2] {'tp_0','tp_1'}, dimensions={0} | all-to-all | bytes 8388608 | tf_op jit(solution)/shard_map/all_to_all | solution.py:20
  347.4 7.3 %reshape_reshape.3 = bf16[1024,2048]{1,0:T(8,128)(2,1)} reshape(bf16[16,1,32,2,2048]{4,3,2,1,0:T(2,128)(2,1)} %all_to_all.29) | data formatting | bytes 8388608 | tf_op jit(solution)/shard_map/reshape;reshape | solution.py:293
  354.7 4.5 fusion.14
  359.2 9.1 %convolution_convert_fusion = bf16[1024,2048]{1,0:T(8,128)(2,1)} fusion(bf16[1024,2048]{1,0:T(8,128)(2,1)} %reshape_reshape.3, bf16[1,256,2048]{2,1,0:T(8,128)(2,1)S(1)} %copy-done, bf16[1,2048,256]{2,1,0:T(8,128)(2,1)} %param.40, f32[1024,256]{1,0:T(8,128)} %fusion.14), kind=kOutput, calls=%fused_computation.10 | convolution fusion | flops 2151153664 | bytes 11534336 | tf_op jit(solution)/shard_map/dot_general | solution.py:297
  368.3 7.6 %convert_element_type.713 = bf16[16,32,2,2048]{3,2,1,0:T(2,128)(2,1)} reshape(bf16[1024,2048]{1,0:T(8,128)(2,1)} %convolution_convert_fusion) | data formatting | bytes 8388608 | tf_op jit(solution)/shard_map/convert_element_type | solution.py:301
  375.9 6.0 %copy.156 = bf16[16,32,2,2048]{3,1,2,0:T(8,128)(2,1)} copy(bf16[16,32,2,2048]{3,2,1,0:T(2,128)(2,1)} %convert_element_type.713) | data formatting | bytes 8388608 | tf_op jit(solution)/shard_map/convert_element_type | solution.py:301
  382.0 58.6 %reduce-scatter.2.cloned.1.call-done = bf16[1,32,2,2048]{3,1,2,0:T(8,128)(2,1)} async-done(((bf16[16,32,2,2048]{3,1,2,0:T(8,128)(2,1)}), bf16[1,32,2,2048]{3,1,2,0:T(8,128)(2,1)}) %reduce-scatter.2.cloned.1.call-update) | async-done | bytes 262160 | tf_op jit(solution)/shard_map/reduce_scatter | solution.py:300
  440.6 1.9 copy.157
  442.5 9.9 %all-to-all-start.3 = ((bf16[32,2,2048]{2,1,0:T(2,128)(2,1)}), bf16[32,2,2048]{2,1,0:T(2,128)(2,1)S(1)}, u32[]{:S(2)}, u32[]{:S(2)}) async-start(bf16[32,2,2048]{2,1,0:T(2,128)(2,1)} %copy.157), calls=%async_computation.4 | async-start | bytes 524288 | tf_op jit(solution)/shard_map/all_to_all | solution.py:307
  452.5 11.1 %all-to-all-done.3 = bf16[32,2,2048]{2,1,0:T(2,128)(2,1)S(1)} async-done(((bf16[32,2,2048]{2,1,0:T(2,128)(2,1)}), bf16[32,2,2048]{2,1,0:T(2,128)(2,1)S(1)}, u32[]{:S(2)}, u32[]{:S(2)}) %all-to-all-start.3) | async-done | bytes 262176 | tf_op jit(solution)/shard_map/all_to_all | solution.py:307
  (133 shorter events, 26.8 us)
Async XLA Ops:
  6.5 352.6 %copy-start = (bf16[1,256,2048]{2,1,0:T(8,128)(2,1)S(1)}, bf16[1,256,2048]{2,1,0:T(8,128)(2,1)}, u32[]{:S(2)}) copy-start(bf16[1,256,2048]{2,1,0:T(8,128)(2,1)} %param.41) | copy-start | bytes 3145732
  6.5 195.4 %all-gather.6.cloned.1.call-start = ((), (), s32[]{:S(2)}) async-start(), calls=%async_computation.5 | async-start | bytes 2359296 | tf_op jit(solution)/shard_map/all_gather | solution.py:71
  9.7 54.5 %collective-permute-start = (bf16[2,512]{0,1:T(8,128)(2,1)S(1)}, bf16[2,512]{0,1:T(8,128)(2,1)S(1)}, u32[]{:S(2)}, u32[]{:S(2)}) collective-permute-start(bf16[2,512]{0,1:T(8,128)(2,1)S(1)} %get-tuple-element.275), channel_id=1, source_target_pairs={{0,16},{16,32},{32,48},{48,64},{64,80},{80,96},{96,112},{112,128},... | collective-permute-start | bytes 6152 | tf_op jit(solution)/shard_map/ppermute | solution.py:32
  12.8 51.4 %collective-permute-start.1 = (bf16[2,512]{0,1:T(8,128)(2,1)S(1)}, bf16[2,512]{0,1:T(8,128)(2,1)S(1)}, u32[]{:S(2)}, u32[]{:S(2)}) collective-permute-start(bf16[2,512]{0,1:T(8,128)(2,1)S(1)} %get-tuple-element.276), channel_id=1, source_target_pairs={{16,0},{32,16},{48,32},{64,48},{80,64},{96,80},{112,96},{128,112},... | collective-permute-start | bytes 6152 | tf_op jit(solution)/shard_map/ppermute | solution.py:34
  17.8 46.2 %copy-start.5 = (f32[2,4]{1,0:T(2,128)}, f32[2,4]{1,0:T(2,128)S(1)}, u32[]{:S(2)}) copy-start(f32[2,4]{1,0:T(2,128)S(1)} %get-tuple-element.240) | copy-start | bytes 100
  62.3 14.6 %copy-start.7 = (f32[4]{0:T(128)}, f32[4]{0:T(128)S(1)}, u32[]{:S(2)}) copy-start(f32[4]{0:T(128)S(1)} %get-tuple-element.308) | copy-start | bytes 52
  62.3 14.6 %copy-start.8 = (f32[4]{0:T(128)}, f32[4]{0:T(128)S(1)}, u32[]{:S(2)}) copy-start(f32[4]{0:T(128)S(1)} %get-tuple-element.309) | copy-start | bytes 52
  62.3 14.6 %copy-start.9 = (f32[4]{0:T(128)}, f32[4]{0:T(128)S(1)}, u32[]{:S(2)}) copy-start(f32[4]{0:T(128)S(1)} %get-tuple-element.310) | copy-start | bytes 52
  62.3 14.6 %copy-start.10 = (f32[4]{0:T(128)}, f32[4]{0:T(128)S(1)}, u32[]{:S(2)}) copy-start(f32[4]{0:T(128)S(1)} %get-tuple-element.311) | copy-start | bytes 52
  66.5 0.7 copy-start.2
  67.2 40.7 %copy-start.11 = (f32[4]{0:T(128)S(1)}, f32[4]{0:T(128)}, u32[]{:S(2)}) copy-start(f32[4]{0:T(128)} %get-tuple-element.313) | copy-start | bytes 52
  67.2 40.7 %copy-start.12 = (f32[4]{0:T(128)S(1)}, f32[4]{0:T(128)}, u32[]{:S(2)}) copy-start(f32[4]{0:T(128)} %get-tuple-element.314) | copy-start | bytes 52
  67.2 40.7 %copy-start.13 = (f32[4]{0:T(128)S(1)}, f32[4]{0:T(128)}, u32[]{:S(2)}) copy-start(f32[4]{0:T(128)} %get-tuple-element.315) | copy-start | bytes 52
  67.2 40.7 %copy-start.14 = (f32[4]{0:T(128)S(1)}, f32[4]{0:T(128)}, u32[]{:S(2)}) copy-start(f32[4]{0:T(128)} %get-tuple-element.316) | copy-start | bytes 52
  67.5 29.1 %copy-start.1 = (f32[2,1,4,64,128]{4,3,2,1,0:T(8,128)}, f32[2,1,4,64,128]{4,3,2,1,0:T(8,128)S(1)}, u32[]{:S(2)}) copy-start(f32[2,1,4,64,128]{4,3,2,1,0:T(8,128)S(1)} %get-tuple-element.138) | copy-start | bytes 786436
  96.2 11.7 %copy-start.3 = (bf16[2,128,4,64]{1,0,3,2:T(2,128)(2,1)}, bf16[2,128,4,64]{1,0,3,2:T(2,128)(2,1)S(1)}, u32[]{:S(2)}) copy-start(bf16[2,128,4,64]{1,0,3,2:T(2,128)(2,1)S(1)} %reshape.1005) | copy-start | bytes 393220
  132.7 87.4 %copy-start.4 = (bf16[16,2048]{1,0:T(8,128)(2,1)S(1)}, bf16[16,2048]{1,0:T(8,128)(2,1)}, u32[]{:S(2)}) copy-start(bf16[16,2048]{1,0:T(8,128)(2,1)} %param.23) | copy-start | bytes 196612
  132.8 87.6 %copy-start.6 = (f32[2048]{0:T(1024)S(1)}, f32[2048]{0:T(1024)}, u32[]{:S(2)}) copy-start(f32[2048]{0:T(1024)} %param.36) | copy-start | bytes 24580
  205.2 15.0 %all-to-all-start = ((bf16[16,16,128]{2,1,0:T(8,128)(2,1)}), bf16[16,16,128]{2,1,0:T(8,128)(2,1)S(1)}, u32[]{:S(2)}, u32[]{:S(2)}) async-start(bf16[16,16,128]{2,1,0:T(8,128)(2,1)} %bitcast.67), calls=%async_computation | async-start | bytes 131072 | tf_op jit(solution)/shard_map/all_to_all | solution.py:265
  215.2 225.4 %reduce-scatter.2.cloned.1.call-start = ((), (), s32[]{:S(2)}) async-start(), calls=%async_computation.6 | async-start | bytes 4456448 | tf_op jit(solution)/shard_map/reduce_scatter | solution.py:300
  347.4 7.3 %copy-start.16 = (bf16[1,2048,256]{2,1,0:T(8,128)(2,1)S(1)}, bf16[1,2048,256]{2,1,0:T(8,128)(2,1)}, u32[]{:S(2)}) copy-start(bf16[1,2048,256]{2,1,0:T(8,128)(2,1)} %param.39) | copy-start | bytes 3145732
  381.9 70.5 %copy-start.15 = (f32[16,2]{0,1:T(2,128)S(1)}, f32[16,2]{0,1:T(2,128)}, u32[]{:S(2)}) copy-start(f32[16,2]{0,1:T(2,128)} %param.38) | copy-start | bytes 388
  442.5 21.1 %all-to-all-start.3 = ((bf16[32,2,2048]{2,1,0:T(2,128)(2,1)}), bf16[32,2,2048]{2,1,0:T(2,128)(2,1)S(1)}, u32[]{:S(2)}, u32[]{:S(2)}) async-start(bf16[32,2,2048]{2,1,0:T(2,128)(2,1)} %copy.157), calls=%async_computation.4 | async-start | bytes 524288 | tf_op jit(solution)/shard_map/all_to_all | solution.py:307
Sparse Core Ops, SparseCore 0:
  167.2 34.6 all-gather.5
  382.1 58.4 reduce-scatter.1
